TPU v7x, 128 devices: a whole 4x4x4 slice. The times are simulated.
128 devices in a mesh: sp: 32 (over z, y, core), tp: 4 (over x).
Axes of the slice: x: 4, y: 4, z: 4, core: 2. Of those that a mesh axis runs over, the one named last changes fastest.
Arguments:
- stream: bfloat16 [8192, 2048], P('sp', 'tp'), may hold values from -1200 to 1200, as said below
- mix_gain: bfloat16 [2048], P('tp'), may hold values from 0.099609375 to 1.8984375
- pool_weight: bfloat16 [4, 512, 512], P('tp'), may hold values from -0.25 to 0.25
- pool_scale: bfloat16 [2048], P('tp'), may hold values from 0.099609375 to 1.8984375
- ffn_gain: bfloat16 [2048], replicated, may hold values from 0.099609375 to 1.8984375
- routes: int32 [8192, 2], P(('sp', 'tp')), may hold values from 0 to 31, all different within a row; in each aligned block of 64 rows (0 to 63, 64 to 127, ...) at most 8 rows name the same one
- route_weight: float32 [8192, 2], P(('sp', 'tp')), may hold values from 0.1 to 1
- w_gate: bfloat16 [32, 2048, 7168], P('sp', None, 'tp'), may hold values from -0.125 to 0.125
- w_up: bfloat16 [32, 2048, 7168], P('sp', None, 'tp'), may hold values from -0.125 to 0.125
- w_down: bfloat16 [32, 7168, 2048], P('sp', 'tp'), may hold values from -0.0625 to 0.0625
Outputs:
- layer_out: bfloat16 [8192, 2048], P(('sp', 'tp'))
Inputs may be any that keep to these rules, and one draw needn't show every extreme that they name: `routes`: each row names 2 different experts. Within each aligned block of 64 rows (the rows of one device) no expert is named by more than 8 rows, a bound that some block reaches. `stream`: finite values.
All inputs are finite; a program needn't handle non-finite values.
Results may differ from a plain program's by a relative error of at most 0.0061.
Values may be sent and summed in bfloat16 or wider, within the bound.
A program may use at most 128 MiB of HBM per device.

v0:
```python
import jax
import jax.numpy as jnp
from jax import lax
from jax.sharding import PartitionSpec as P

NORM_EPS = 1e-06


def split_up(array, dim, count):
    before, after = (array.shape[:dim], array.shape[dim + 1 :])
    return jnp.moveaxis(array.reshape(*before, count, -1, *after), dim, 0)


def sent_and_summed(array, axis, dim):
    blocks = split_up(array, dim, lax.axis_size(axis))
    arrived = lax.all_to_all(blocks, axis, split_axis=0, concat_axis=0, tiled=True)
    return arrived.astype(jnp.float32).sum(axis=0)


def sent_to_all(array, axis):
    copies = jnp.broadcast_to(array, (lax.axis_size(axis), *array.shape))
    return lax.all_to_all(copies, axis, split_axis=0, concat_axis=0, tiled=True)


def of_everyone(array, axis):
    return sent_to_all(array, axis).sum(axis=0)


def passed_along(block, axis, distance):
    devices = range(lax.axis_size(axis))
    route = [(i - distance, i) for i in devices if i - distance in devices]
    return lax.ppermute(block, axis, route)


def expert_rows(arrived, w_gate, w_up, w_down):
    sp_count, tp_count, slot_count, model_width = arrived.shape
    flat_rows = arrived.reshape(-1, model_width)
    gate_val = jnp.dot(flat_rows, w_gate[0], preferred_element_type=jnp.float32)
    up_val = jnp.dot(flat_rows, w_up[0], preferred_element_type=jnp.float32)
    hidden = (jax.nn.silu(gate_val) * up_val).astype(jnp.bfloat16)
    block_out = jnp.dot(hidden, w_down[0], preferred_element_type=jnp.float32)
    block_out = block_out.reshape(sp_count, tp_count, slot_count, model_width)
    summed = sent_and_summed(block_out.astype(jnp.bfloat16), "tp", 1)
    return summed.astype(jnp.bfloat16).reshape(sp_count, slot_count, model_width)


def per_device(
    stream, mix_gain, pool_weight, pool_scale, ffn_gain, routes, route_weight, w_gate, w_up, w_down
):
    tok_rows, shard_width = stream.shape
    tp_count = lax.axis_size("tp")
    sp_count = lax.axis_size("sp")
    model_width = shard_width * tp_count
    stream_f32 = stream.astype(jnp.float32)
    square = of_everyone(jnp.sum(stream_f32 * stream_f32, axis=1), "tp")
    row_scale = lax.rsqrt(square / model_width + NORM_EPS)[:, None]
    normed = (stream_f32 * row_scale * mix_gain.astype(jnp.float32)).astype(jnp.bfloat16)
    local_groups = pool_weight.shape[0]
    halo_rows = 2 ** (local_groups * tp_count) - 1
    previous = passed_along(normed[tok_rows - halo_rows :], "sp", 1)
    extended = jnp.concatenate([previous, normed], axis=0)
    first_row = lax.axis_index("sp") * tok_rows
    position = first_row + jnp.arange(tok_rows, dtype=jnp.int32)
    source = first_row - halo_rows + jnp.arange(tok_rows + halo_rows, dtype=jnp.int32)
    lag_rows = position[:, None] - source[None, :]
    group_index = lax.axis_index("tp") * local_groups + 0
    window_len = jnp.left_shift(jnp.int32(2), group_index)
    band_mask = ((lag_rows >= 0) & (lag_rows < window_len)).astype(jnp.bfloat16)
    window_sum = jnp.dot(band_mask, extended, preferred_element_type=jnp.float32)
    window_count = jnp.minimum(position + 1, window_len).astype(jnp.float32)[:, None]
    own_rows = normed.astype(jnp.float32)
    pooled = (window_sum / window_count - own_rows).astype(jnp.bfloat16)
    group_outs = jnp.dot(pooled, pool_weight[0], preferred_element_type=jnp.float32)
    mixer_out = group_outs * pool_scale.astype(jnp.float32)
    after_mix = (stream_f32 + mixer_out).astype(jnp.bfloat16)
    token_rows = lax.all_to_all(after_mix, "tp", split_axis=0, concat_axis=1, tiled=True)
    after_f32 = token_rows.astype(jnp.float32)
    ffn_scale = lax.rsqrt(jnp.mean(after_f32 * after_f32, axis=1, keepdims=True) + NORM_EPS)
    normed2 = (after_f32 * ffn_scale * ffn_gain.astype(jnp.float32)).astype(jnp.bfloat16)
    tok_count, top_count = routes.shape
    capacity = 2 * tok_count * top_count // sp_count
    flat_routes = routes.reshape(-1)
    is_expert = (flat_routes[:, None] == jnp.arange(sp_count, dtype=jnp.int32)[None, :]).astype(
        jnp.int32
    )
    slot_rank = jnp.cumsum(is_expert, axis=0) - is_expert
    slot_index = jnp.sum(slot_rank * is_expert, axis=1)
    dest_slot = (flat_routes * capacity + slot_index).reshape(tok_count, top_count)
    slot_ids = jnp.arange(sp_count * capacity, dtype=jnp.int32)
    pick_masks = [
        (dest_slot[:, pick_index][None, :] == slot_ids[:, None]).astype(jnp.bfloat16)
        for pick_index in range(top_count)
    ]
    dispatch_mask = pick_masks[0]
    pick_index = 1
    dispatch_mask = dispatch_mask + pick_masks[pick_index]
    send_rows = jnp.dot(dispatch_mask, normed2, preferred_element_type=jnp.float32).astype(
        jnp.bfloat16
    )
    send_rows = send_rows.reshape(sp_count, capacity, model_width)
    copies = jnp.broadcast_to(send_rows[:, None], (sp_count, tp_count, capacity, model_width))
    copies = copies.reshape(sp_count * tp_count, capacity, model_width)
    arrived = lax.all_to_all(copies, ("sp", "tp"), split_axis=0, concat_axis=0, tiled=True)
    shaped = arrived.reshape(sp_count, tp_count, arrived.shape[1], model_width)
    served = expert_rows(shaped, w_gate, w_up, w_down)
    returned = lax.all_to_all(served, "sp", split_axis=0, concat_axis=0, tiled=True).reshape(
        sp_count * capacity, model_width
    )
    expert_sum = after_f32
    for pick_index in range(top_count):
        picked_out = jnp.dot(pick_masks[pick_index].T, returned, preferred_element_type=jnp.float32)
        expert_sum = expert_sum + route_weight[:, pick_index : pick_index + 1] * picked_out
    return expert_sum.astype(jnp.bfloat16)


def solution(mesh):
    in_specs = (
        P("sp", "tp"),
        P("tp"),
        P("tp", None, None),
        P("tp"),
        P(),
        P(("sp", "tp"), None),
        P(("sp", "tp"), None),
        P("sp", None, "tp"),
        P("sp", None, "tp"),
        P("sp", "tp", None),
    )
    out_specs = P(("sp", "tp"), None)
    return jax.shard_map(
        per_device, mesh=mesh, in_specs=in_specs, out_specs=out_specs, check_vma=False
    )
```

profile of v0, /device:TPU:1, one launch (start us, length us, event | category | flops | bytes accessed | tf_op | source)
XLA Modules:
  0.0 202.0 jit_solution(1521831828139508031)
XLA Ops:
  0.0 1.1 fusion.23
  1.1 0.6 broadcast_in_dim.6
  1.7 4.8 %all-to-all-start = ((f32[4,1,256]{2,1,0:T(1,128)}), f32[4,1,256]{2,1,0:T(1,128)S(1)}, u32[]{:S(2)}, u32[]{:S(2)}) async-start(f32[4,1,256]{2,1,0:T(1,128)} %broadcast_in_dim.6), calls=%async_computation | async-start | bytes 8192 | tf_op jit(solution)/shard_map/all_to_all | solution.py:22
  6.6 0.8 copy.37
  7.3 0.1 eq.45
  7.6 0.2 reduce_window_sum.11
  7.7 0.2 select_reduce_fusion
  7.9 0.1 reduce_sum.53
  8.1 0.7 multiply_add_fusion
  8.8 0.7 convert_element_type.72
  9.5 1.2 all-to-all-done
  10.8 1.1 fusion.25
  11.9 5.2 %collective-permute-start = (bf16[15,512]{1,0:T(8,128)(2,1)S(1)}, bf16[15,512]{1,0:T(8,128)(2,1)S(1)}, u32[]{:S(2)}, u32[]{:S(2)}) collective-permute-start(bf16[15,512]{1,0:T(8,128)(2,1)S(1)} %slice.20), channel_id=1, source_target_pairs={{0,4},{4,8},{8,12},{12,16},{16,20},{20,24},{24,28},{28,32},{32,36}... | collective-permute-start | bytes 46088 | tf_op jit(solution)/shard_map/ppermute | solution.py:32
  17.1 0.7 convert_element_type.77
  17.8 0.7 convert_element_type.86
  18.4 2.2 %fusion.18 = bf16[256,512]{1,0:T(8,128)(2,1)} fusion(bf16[256,512]{1,0:T(8,128)(2,1)} %param.10, bf16[1,512,512]{2,1,0:T(8,128)(2,1)S(1)} %copy-done, bf16[256,512]{1,0:T(8,128)(2,1)S(1)} %fusion.25, bf16[15,512]{1,0:T(8,128)(2,1)S(1)} %collective-permute-done, f32[512]{0:T(512)S(1)} %convert_element_type.77, f32[256]{0:T(256)S(1)} %get-tuple-element.9, ...), kind=kOutput, calls=%fused_computation.21 | convolution fusion | flops 207139840 | bytes 1331264 | tf_op jit(solution)/shard_map/dot_general | solution.py:73
  20.7 3.4 %all-to-all-start.1 = ((bf16[4,64,512]{2,1,0:T(8,128)(2,1)}), bf16[4,64,512]{2,1,0:T(8,128)(2,1)S(1)}, u32[]{:S(2)}, u32[]{:S(2)}) async-start(bf16[4,64,512]{2,1,0:T(8,128)(2,1)} %bitcast.1), calls=%async_computation.1 | async-start | bytes 524288 | tf_op jit(solution)/shard_map/all_to_all | solution.py:76
  24.1 5.6 %all-to-all-done.1 = bf16[4,64,512]{2,1,0:T(8,128)(2,1)S(1)} async-done(((bf16[4,64,512]{2,1,0:T(8,128)(2,1)}), bf16[4,64,512]{2,1,0:T(8,128)(2,1)S(1)}, u32[]{:S(2)}, u32[]{:S(2)}) %all-to-all-start.1) | async-done | bytes 262176 | tf_op jit(solution)/shard_map/all_to_all | solution.py:76
  29.8 0.2 fusion.22
  29.9 0.5 fusion.12
  30.4 0.5 broadcast_in_dim.8
  31.0 63.0 %all_to_all.34 = bf16[128,8,2048]{2,1,0:T(8,128)(2,1)S(1)} all-to-all(bf16[128,8,2048]{2,1,0:T(8,128)(2,1)S(1)} %bitcast.52), channel_id=1, replica_groups=mesh['sp'=32,'tp'=4] {'sp','tp'}, dimensions={0} | all-to-all | bytes 8388608 | tf_op jit(solution)/shard_map/all_to_all | solution.py:103
  94.0 9.8 %fusion.4 = f32[1024,1792]{1,0:T(8,128)} fusion(bf16[1,2048,1792]{2,1,0:T(8,128)(2,1)S(1)} %bitcast.56, bf16[128,8,2048]{2,1,0:T(8,128)(2,1)S(1)} %all_to_all.34), kind=kOutput, calls=%fused_computation.4 | convolution fusion | flops 7516192768 | bytes 18874368 | tf_op jit(solution)/shard_map/dot_general | solution.py:38
  103.9 10.2 %multiply_convert_fusion = bf16[1024,1792]{1,0:T(8,128)(2,1)S(1)} fusion(f32[1024,1792]{1,0:T(8,128)} %fusion.4, bf16[1,2048,1792]{2,1,0:T(8,128)(2,1)S(1)} %bitcast.58, bf16[128,8,2048]{2,1,0:T(8,128)(2,1)S(1)} %all_to_all.34), kind=kOutput, calls=%fused_computation.6 | convolution fusion | flops 7527202816 | bytes 22544384 | tf_op jit(solution)/shard_map/dot_general | solution.py:39
  114.2 7.9 %convert_bitcast_fusion = bf16[4,32,1,8,2048]{4,3,0,1,2:T(8,128)(2,1)S(1)} fusion(bf16[32,4,8,1792]{3,2,1,0:T(8,128)(2,1)S(1)} %bitcast.61, bf16[1,1792,2048]{2,1,0:T(8,128)(2,1)S(1)} %bitcast.60), kind=kOutput, calls=%fused_computation.9 | convolution fusion | flops 7518289920 | bytes 15204352 | tf_op jit(solution)/shard_map/dot_general | solution.py:41
  122.1 0.3 copy.39
  122.4 51.8 %all_to_all.35 = bf16[4,32,1,8,2048]{4,3,1,2,0:T(8,128)(2,1)} all-to-all(bf16[4,32,1,8,2048]{4,3,1,2,0:T(8,128)(2,1)S(1)} %copy.39), channel_id=1, replica_groups=mesh['sp'=32,'tp'=4] {'tp'}, dimensions={0} | all-to-all | bytes 8388608 | tf_op jit(solution)/shard_map/all_to_all | solution.py:16
  174.3 4.3 %reduce_sum.55 = bf16[32,8,2048]{2,1,0:T(8,128)(2,1)} reduce(bf16[4,32,1,8,2048]{4,3,1,2,0:T(8,128)(2,1)} %all_to_all.35, bf16[]{:T(256)} %constant.41.clone.1), dimensions={0,2}, to_apply=%region_5.6 | reduce | flops 1572864 | bytes 5242882 | tf_op jit(solution)/shard_map/reduce_sum | solution.py:17
  178.5 4.9 %all-to-all-start.4 = ((bf16[32,8,2048]{2,1,0:T(8,128)(2,1)}), bf16[32,8,2048]{2,1,0:T(8,128)(2,1)S(1)}, u32[]{:S(2)}, u32[]{:S(2)}) async-start(bf16[32,8,2048]{2,1,0:T(8,128)(2,1)} %reduce_sum.55), calls=%async_computation.4 | async-start | bytes 2097152 | tf_op jit(solution)/shard_map/all_to_all | solution.py:106
  183.5 17.1 %all-to-all-done.4 = bf16[32,8,2048]{2,1,0:T(8,128)(2,1)S(1)} async-done(((bf16[32,8,2048]{2,1,0:T(8,128)(2,1)}), bf16[32,8,2048]{2,1,0:T(8,128)(2,1)S(1)}, u32[]{:S(2)}, u32[]{:S(2)}) %all-to-all-start.4) | async-done | bytes 1048608 | tf_op jit(solution)/shard_map/all_to_all | solution.py:106
  200.6 0.3 convolution_multiply_fusion
  200.9 1.1 fusion.15
  (32 shorter events, 0.4 us)
Async XLA Ops:
  0.0 18.4 %copy-start = (bf16[1,512,512]{2,1,0:T(8,128)(2,1)S(1)}, bf16[1,512,512]{2,1,0:T(8,128)(2,1)}, u32[]{:S(2)}) copy-start(bf16[1,512,512]{2,1,0:T(8,128)(2,1)} %param.12) | copy-start | bytes 1572868
  1.7 9.0 %all-to-all-start = ((f32[4,1,256]{2,1,0:T(1,128)}), f32[4,1,256]{2,1,0:T(1,128)S(1)}, u32[]{:S(2)}, u32[]{:S(2)}) async-start(f32[4,1,256]{2,1,0:T(1,128)} %broadcast_in_dim.6), calls=%async_computation | async-start | bytes 8192 | tf_op jit(solution)/shard_map/all_to_all | solution.py:22
  11.9 6.6 %collective-permute-start = (bf16[15,512]{1,0:T(8,128)(2,1)S(1)}, bf16[15,512]{1,0:T(8,128)(2,1)S(1)}, u32[]{:S(2)}, u32[]{:S(2)}) collective-permute-start(bf16[15,512]{1,0:T(8,128)(2,1)S(1)} %slice.20), channel_id=1, source_target_pairs={{0,4},{4,8},{8,12},{12,16},{16,20},{20,24},{24,28},{28,32},{32,36}... | collective-permute-start | bytes 46088 | tf_op jit(solution)/shard_map/ppermute | solution.py:32
  20.7 9.0 %all-to-all-start.1 = ((bf16[4,64,512]{2,1,0:T(8,128)(2,1)}), bf16[4,64,512]{2,1,0:T(8,128)(2,1)S(1)}, u32[]{:S(2)}, u32[]{:S(2)}) async-start(bf16[4,64,512]{2,1,0:T(8,128)(2,1)} %bitcast.1), calls=%async_computation.1 | async-start | bytes 524288 | tf_op jit(solution)/shard_map/all_to_all | solution.py:76
  29.9 64.1 %slice-start = ((s8[7340032]{0:T(1024)(128)(4,1)}), s8[4194304]{0:T(1024)(128)(4,1)S(1)}, s32[]{:S(2)}) async-start(s8[7340032]{0:T(1024)(128)(4,1)} %bitcast.55), calls=%async_computation.5 | async-start | bytes 8388608
  30.9 63.1 %slice-start.1 = ((s8[7340032]{0:T(1024)(128)(4,1)}), s8[3145728]{0:T(1024)(128)(4,1)S(1)}, s32[]{:S(2)}) async-start(s8[7340032]{0:T(1024)(128)(4,1)} %bitcast.55), calls=%async_computation.6 | async-start | bytes 6291456
  31.0 72.9 %slice-start.2 = ((s8[7340032]{0:T(1024)(128)(4,1)}), s8[4194304]{0:T(1024)(128)(4,1)S(1)}, s32[]{:S(2)}) async-start(s8[7340032]{0:T(1024)(128)(4,1)} %bitcast.57), calls=%async_computation.7 | async-start | bytes 8388608
  94.0 9.9 %slice-start.3 = ((s8[7340032]{0:T(1024)(128)(4,1)}), s8[3145728]{0:T(1024)(128)(4,1)S(1)}, s32[]{:S(2)}) async-start(s8[7340032]{0:T(1024)(128)(4,1)} %bitcast.57), calls=%async_computation.8 | async-start | bytes 6291456
  94.0 20.1 %slice-start.4 = ((s8[7340032]{0:T(1024)(128)(4,1)}), s8[4194304]{0:T(1024)(128)(4,1)S(1)}, s32[]{:S(2)}) async-start(s8[7340032]{0:T(1024)(128)(4,1)} %bitcast.59), calls=%async_computation.9 | async-start | bytes 8388608
  103.9 10.3 %slice-start.5 = ((s8[7340032]{0:T(1024)(128)(4,1)}), s8[3145728]{0:T(1024)(128)(4,1)S(1)}, s32[]{:S(2)}) async-start(s8[7340032]{0:T(1024)(128)(4,1)} %bitcast.59), calls=%async_computation.10 | async-start | bytes 6291456
  122.4 61.0 %copy-start.1 = (f32[64,2]{0,1:T(2,128)S(1)}, f32[64,2]{0,1:T(2,128)}, u32[]{:S(2)}) copy-start(f32[64,2]{0,1:T(2,128)} %param.16) | copy-start | bytes 1540
  178.5 22.1 %all-to-all-start.4 = ((bf16[32,8,2048]{2,1,0:T(8,128)(2,1)}), bf16[32,8,2048]{2,1,0:T(8,128)(2,1)S(1)}, u32[]{:S(2)}, u32[]{:S(2)}) async-start(bf16[32,8,2048]{2,1,0:T(8,128)(2,1)} %reduce_sum.55), calls=%async_computation.4 | async-start | bytes 2097152 | tf_op jit(solution)/shard_map/all_to_all | solution.py:106
where the time goes:
time: 203 us; the launch traced here: 202 us
  blocking collectives  115 us (57%)
  matrix products  32.1 us (16%)
  waiting for transfers between devices  23.9 us (12%)
  starting transfers between devices  18.4 us (9%)
  other arithmetic  9.91 us (5%)
  local copies, waits for them, and re-layouts  2.65 us (1%)
    all_to_all x1, blocking collectives, per_device(): lax.all_to_all(copies, ('sp', 'tp'), split_axis=0, concat_axis=0, tiled=T...  63 us
    all_to_all x1, blocking collectives, sent_and_summed(): lax.all_to_all(blocks, axis, split_axis=0, concat_axis=0, tiled=True)  51.8 us
    all_to_all x1, waiting for transfers between devices, per_device(): lax.all_to_all(served, 'sp', split_axis=0, concat_axis=0, tiled=True)  17.1 us
    dot_general x1, matrix products, expert_rows(): up_val = jnp.dot(flat_rows, w_up[0], preferred_element_type=jnp.float32)  10.2 us
    dot_general x1, matrix products, expert_rows(): gate_val = jnp.dot(flat_rows, w_gate[0], preferred_element_type=jnp.float32)  9.83 us
    dot_general x1, matrix products, expert_rows(): block_out = jnp.dot(hidden, w_down[0], preferred_element_type=jnp.float32)  7.93 us
    all_to_all x1, waiting for transfers between devices, per_device(): lax.all_to_all(after_mix, 'tp', split_axis=0, concat_axis=1, tiled=True)  5.55 us
    ppermute x1, starting transfers between devices, passed_along(): return lax.ppermute(block, axis, route)  5.19 us
  transfers between devices with their start and end apart: 4, of which 3 were waited for; matrix products, arithmetic and copies ran while one was open for 2% of the time, Pallas kernels for 0%

commit v1 on v0

v1 whole, which is shorter than its diff:
```python
import functools

import jax
import jax.numpy as jnp
from jax import lax
from jax.experimental import pallas as pl
from jax.experimental.pallas import tpu as pltpu
from jax.sharding import PartitionSpec as P

NORM_EPS = 1e-06
MESH = pl.DeviceIdType.MESH
STEPS = (0, 1, 3, 2)
CHUNKS = 4
PEERS = 8
TILE = 256


def split_up(array, dim, count):
    before, after = (array.shape[:dim], array.shape[dim + 1 :])
    return jnp.moveaxis(array.reshape(*before, count, -1, *after), dim, 0)


def sent_to_all(array, axis):
    copies = jnp.broadcast_to(array, (lax.axis_size(axis), *array.shape))
    return lax.all_to_all(copies, axis, split_axis=0, concat_axis=0, tiled=True)


def of_everyone(array, axis):
    return sent_to_all(array, axis).sum(axis=0)


def passed_along(block, axis, distance):
    devices = range(lax.axis_size(axis))
    route = [(i - distance, i) for i in devices if i - distance in devices]
    return lax.ppermute(block, axis, route)


def relative_place(expert, sp):
    dz = (expert // 8 - sp // 8 + 4) % 4
    dy = (expert // 2 % 4 - sp // 2 % 4 + 4) % 4
    dc = (expert + sp) % 2
    def place(d):
        return jnp.where(d == 2, 3, jnp.where(d == 3, 2, d))
    return place(dz) * PEERS + place(dy) * 2 + dc


def experts_kernel(
    s_ref, wg_hbm, wu_hbm, wd_hbm, r_ref,
    x_buf, wg, wu, wd, hid, part, relay_l, relay_r, from_l, from_r, sums,
    w_sem, d_ssem, d_rsem, g_ssem, g_rsem, p_ssem, p_rsem, r_ssem, r_rsem,
):
    sp = lax.axis_index("sp")
    tp = lax.axis_index("tp")
    z, y, core = sp // 8, sp // 2 % 4, sp % 2
    left, right = (sp, (tp + 3) % 4), (sp, (tp + 1) % 4)
    width = wd.shape[0] * TILE
    up_tiles, down_tiles = wg.shape[0], wd.shape[0]

    w_up_copies, w_down_copies = [], []
    for j in range(up_tiles):
        cols = pl.ds(j * TILE, TILE)
        for i, (src, dst) in enumerate(((wg_hbm, wg), (wu_hbm, wu))):
            w_up_copies.append(
                pltpu.make_async_copy(src.at[0, :, cols], dst.at[j], w_sem.at[2 * j + i])
            )
    for j in range(down_tiles):
        w_down_copies.append(
            pltpu.make_async_copy(
                wd_hbm.at[0, :, pl.ds(j * TILE, TILE)], wd.at[j], w_sem.at[2 * up_tiles + j]
            )
        )

    barrier = pltpu.get_barrier_semaphore()

    def peer(k, sign):
        dz, dy, dc = STEPS[k // PEERS], STEPS[k % PEERS // 2], k % 2
        if sign < 0:
            dz, dy = (4 - dz) % 4, (4 - dy) % 4
        return (((z + dz) % 4) * 8 + ((y + dy) % 4) * 2 + (core + dc) % 2, tp)

    for k in range(1, CHUNKS * PEERS):
        pl.semaphore_signal(barrier, inc=1, device_id=peer(k, 1), device_id_type=MESH)
    for neighbour in (left, right):
        pl.semaphore_signal(barrier, inc=1, device_id=neighbour, device_id_type=MESH)
    for copy in w_up_copies + w_down_copies:
        copy.start()
    pl.semaphore_wait(barrier, CHUNKS * PEERS + 1)

    def remote(src, dst, ssem, rsem, target):
        return pltpu.make_async_remote_copy(
            src_ref=src, dst_ref=dst, send_sem=ssem, recv_sem=rsem,
            device_id=target, device_id_type=MESH,
        )

    sent = []
    dispatch = {}
    for k in range(1, CHUNKS * PEERS):
        dispatch[k] = remote(
            s_ref.at[k], x_buf.at[k // PEERS, 0, k % PEERS], d_ssem.at[k], d_rsem.at[k], peer(k, 1)
        )
        dispatch[k].start()
        sent.append(dispatch[k])
    x_buf[0, 0, 0] = s_ref[0]

    def arrived(c):
        for k in range(c * PEERS, (c + 1) * PEERS):
            if k:
                dispatch[k].wait_recv()

    shared = {}

    def share(c):
        shared[c] = (
            remote(x_buf.at[c, 0, pl.ds(0, 4)], x_buf.at[c, 1, pl.ds(0, 4)],
                   g_ssem.at[c, 0], g_rsem.at[c, 0], left),
            remote(x_buf.at[c, 0, pl.ds(4, 4)], x_buf.at[c, 1, pl.ds(4, 4)],
                   g_ssem.at[c, 1], g_rsem.at[c, 1], right),
        )
        for copy in shared[c]:
            copy.start()
            sent.append(copy)

    def up(c):
        for copy in shared[c]:
            copy.wait_recv()
        if c == 0:
            for copy in w_up_copies:
                copy.wait()

        def tile(j, carry):
            rows = x_buf[c].reshape(2 * PEERS * 16, width)
            gate = jnp.dot(rows, wg[j], preferred_element_type=jnp.float32)
            raised = jnp.dot(rows, wu[j], preferred_element_type=jnp.float32)
            hid[j] = (jax.nn.silu(gate) * raised).astype(jnp.bfloat16)
            return carry

        lax.fori_loop(0, up_tiles, tile, 0)

    def down(c):
        if c == 0:
            for copy in w_down_copies:
                copy.wait()

        def tile(j, carry):
            rows = jnp.concatenate([hid[i] for i in range(up_tiles)], axis=1)
            out = jnp.dot(rows, wd[j], preferred_element_type=jnp.float32)
            out = out.reshape(2, PEERS, 2, 8, TILE)
            own, other = out[0], out[1]
            cols = pl.ds(pl.multiple_of(j * TILE, TILE), TILE)
            blocks = (
                own[:, 0],
                own[:, 1],
                jnp.concatenate([other[:4, 0], other[4:, 1]], axis=0),
                jnp.concatenate([other[:4, 1], other[4:, 0]], axis=0),
            )
            for b, block in enumerate(blocks):
                part[c, b, :, cols] = block.reshape(PEERS * 8, TILE).astype(jnp.bfloat16)
            return carry

        lax.fori_loop(0, down_tiles, tile, 0)

    head, tail = pl.ds(0, 32), pl.ds(32, 32)
    moves = {}

    def reduce_first(c):
        moves[c] = [
            remote(part.at[c, 1, head], relay_l.at[c], p_ssem.at[c, 0], p_rsem.at[c, 0], right),
            remote(part.at[c, 1, tail], relay_r.at[c], p_ssem.at[c, 1], p_rsem.at[c, 1], left),
            remote(part.at[c, 2, tail], from_l.at[c, tail], p_ssem.at[c, 2], p_rsem.at[c, 2], right),
            remote(part.at[c, 3, head], from_r.at[c, head], p_ssem.at[c, 3], p_rsem.at[c, 3], left),
            remote(part.at[c, 2, head], from_l.at[c, head], p_ssem.at[c, 4], p_rsem.at[c, 4], right),
            remote(part.at[c, 3, tail], from_r.at[c, tail], p_ssem.at[c, 5], p_rsem.at[c, 5], left),
        ]
        for copy in moves[c][:4]:
            copy.start()
        sent.extend(moves[c])

    def reduce_second(c):
        moves[c][0].wait_recv()
        moves[c][1].wait_recv()

        def tile(j, carry):
            cols = pl.ds(pl.multiple_of(j * TILE, TILE), TILE)
            for b, rows, relay in ((2, head, relay_l), (3, tail, relay_r)):
                total = part[c, b, rows, cols].astype(jnp.float32) + relay[c, :, cols].astype(
                    jnp.float32
                )
                part[c, b, rows, cols] = total.astype(jnp.bfloat16)
            return carry

        lax.fori_loop(0, down_tiles, tile, 0)
        moves[c][4].start()
        moves[c][5].start()

    returns = {}

    def reduce_third(c):
        for copy in moves[c][2:]:
            copy.wait_recv()

        def tile(j, carry):
            cols = pl.ds(pl.multiple_of(j * TILE, TILE), TILE)
            total = (
                part[c, 0, :, cols].astype(jnp.float32)
                + from_l[c, :, cols].astype(jnp.float32)
                + from_r[c, :, cols].astype(jnp.float32)
            )
            sums[c, :, :, cols] = total.reshape(PEERS, 8, TILE).astype(jnp.bfloat16)
            return carry

        lax.fori_loop(0, down_tiles, tile, 0)
        for i in range(PEERS):
            k = c * PEERS + i
            if k:
                returns[k] = remote(
                    sums.at[c, i], r_ref.at[k], r_ssem.at[k], r_rsem.at[k], peer(k, -1)
                )
                returns[k].start()
                sent.append(returns[k])
            else:
                r_ref[0] = sums[0, 0]

    for c in range(2):
        arrived(c)
        share(c)
    for c in range(CHUNKS):
        up(c)
        if c + 2 < CHUNKS:
            arrived(c + 2)
            share(c + 2)
        if c:
            reduce_second(c - 1)
        down(c)
        reduce_first(c)
        if c:
            reduce_third(c - 1)
    reduce_second(CHUNKS - 1)
    reduce_third(CHUNKS - 1)
    for k in range(1, CHUNKS * PEERS):
        returns[k].wait_recv()
    for copy in sent:
        copy.wait_send()


def run_experts(send_rows, w_gate, w_up, w_down):
    width, inner = w_gate.shape[1:]
    up_tiles, down_tiles = inner // TILE, width // TILE
    bf16 = jnp.bfloat16
    dma = pltpu.SemaphoreType.DMA
    count = CHUNKS * PEERS
    return pl.pallas_call(
        experts_kernel,
        name="experts",
        out_shape=jax.ShapeDtypeStruct((count, 8, width), bf16),
        in_specs=[pl.BlockSpec(memory_space=pltpu.VMEM)] + [pl.BlockSpec(memory_space=pl.ANY)] * 3,
        out_specs=pl.BlockSpec(memory_space=pltpu.VMEM),
        scratch_shapes=[
            pltpu.VMEM((CHUNKS, 2, PEERS, 16, width), bf16),
            pltpu.VMEM((up_tiles, width, TILE), bf16),
            pltpu.VMEM((up_tiles, width, TILE), bf16),
            pltpu.VMEM((down_tiles, inner, TILE), bf16),
            pltpu.VMEM((up_tiles, 2 * PEERS * 16, TILE), bf16),
            pltpu.VMEM((CHUNKS, 4, PEERS * 8, width), bf16),
            pltpu.VMEM((CHUNKS, PEERS * 4, width), bf16),
            pltpu.VMEM((CHUNKS, PEERS * 4, width), bf16),
            pltpu.VMEM((CHUNKS, PEERS * 8, width), bf16),
            pltpu.VMEM((CHUNKS, PEERS * 8, width), bf16),
            pltpu.VMEM((CHUNKS, PEERS, 8, width), bf16),
            dma((2 * up_tiles + down_tiles,)),
            dma((count,)), dma((count,)),
            dma((CHUNKS, 2)), dma((CHUNKS, 2)),
            dma((CHUNKS, 6)), dma((CHUNKS, 6)),
            dma((count,)), dma((count,)),
        ],
        compiler_params=pltpu.CompilerParams(
            collective_id=0, has_side_effects=True, vmem_limit_bytes=60 * 2**20
        ),
    )(send_rows, w_gate, w_up, w_down)


def slots_of(routes, sp, sp_count, slots):
    flat = routes.reshape(-1)
    is_expert = (flat[:, None] == jnp.arange(sp_count, dtype=jnp.int32)[None, :]).astype(jnp.int32)
    rank = jnp.cumsum(is_expert, axis=0) - is_expert
    slot = jnp.sum(rank * is_expert, axis=1)
    return relative_place(flat, sp).reshape(routes.shape), slot.reshape(routes.shape)


def per_device(
    stream, mix_gain, pool_weight, pool_scale, ffn_gain, routes, route_weight, w_gate, w_up, w_down
):
    tok_rows, shard_width = stream.shape
    tp_count = lax.axis_size("tp")
    sp_count = lax.axis_size("sp")
    sp = lax.axis_index("sp")
    model_width = shard_width * tp_count
    across = [(i, (i + 2) % tp_count) for i in range(tp_count)]
    routes_across = lax.ppermute(routes, "tp", across)
    stream_f32 = stream.astype(jnp.float32)
    square = of_everyone(jnp.sum(stream_f32 * stream_f32, axis=1), "tp")
    row_scale = lax.rsqrt(square / model_width + NORM_EPS)[:, None]
    normed = (stream_f32 * row_scale * mix_gain.astype(jnp.float32)).astype(jnp.bfloat16)
    local_groups = pool_weight.shape[0]
    halo_rows = 2 ** (local_groups * tp_count) - 1
    previous = passed_along(normed[tok_rows - halo_rows :], "sp", 1)
    extended = jnp.concatenate([previous, normed], axis=0)
    first_row = sp * tok_rows
    position = first_row + jnp.arange(tok_rows, dtype=jnp.int32)
    source = first_row - halo_rows + jnp.arange(tok_rows + halo_rows, dtype=jnp.int32)
    lag_rows = position[:, None] - source[None, :]
    group_index = lax.axis_index("tp") * local_groups + 0
    window_len = jnp.left_shift(jnp.int32(2), group_index)
    band_mask = ((lag_rows >= 0) & (lag_rows < window_len)).astype(jnp.bfloat16)
    window_sum = jnp.dot(band_mask, extended, preferred_element_type=jnp.float32)
    window_count = jnp.minimum(position + 1, window_len).astype(jnp.float32)[:, None]
    own_rows = normed.astype(jnp.float32)
    pooled = (window_sum / window_count - own_rows).astype(jnp.bfloat16)
    group_outs = jnp.dot(pooled, pool_weight[0], preferred_element_type=jnp.float32)
    mixer_out = group_outs * pool_scale.astype(jnp.float32)
    after_mix = (stream_f32 + mixer_out).astype(jnp.bfloat16)
    block_rows = tok_rows // tp_count
    blocks = after_mix.reshape(tp_count, block_rows, shard_width)
    doubled = jnp.stack([blocks, jnp.roll(blocks, -2, axis=0)], axis=1)
    taken = lax.all_to_all(doubled, "tp", split_axis=0, concat_axis=0, tiled=True)
    taken = taken.transpose(1, 2, 0, 3).reshape(2 * block_rows, model_width)
    after_f32 = taken.astype(jnp.float32)
    ffn_scale = lax.rsqrt(jnp.mean(after_f32 * after_f32, axis=1, keepdims=True) + NORM_EPS)
    normed2 = (after_f32 * ffn_scale * ffn_gain.astype(jnp.float32)).astype(jnp.bfloat16)
    tok_count, top_count = routes.shape
    capacity = 2 * tok_count * top_count // sp_count
    own_place, own_slot = slots_of(routes, sp, sp_count, capacity)
    far_place, far_slot = slots_of(routes_across, sp, sp_count, capacity)
    send_ids = jnp.arange(sp_count * 2 * capacity, dtype=jnp.int32)

    def mask_of(place, slot, offset):
        target = place * (2 * capacity) + offset + slot
        hits = target[None, :, :] == send_ids[:, None, None]
        return hits.any(axis=2).astype(jnp.bfloat16)

    dispatch_mask = jnp.concatenate(
        [mask_of(own_place, own_slot, 0), mask_of(far_place, far_slot, capacity)], axis=1
    )
    send_rows = jnp.dot(dispatch_mask, normed2, preferred_element_type=jnp.float32).astype(
        jnp.bfloat16
    )
    send_rows = send_rows.reshape(sp_count, 2 * capacity, model_width)
    returned = run_experts(send_rows, w_gate, w_up, w_down).reshape(
        sp_count * capacity, model_width
    )
    slot_ids = jnp.arange(sp_count * capacity, dtype=jnp.int32)
    dest = own_place * capacity + own_slot
    expert_sum = after_f32[:block_rows]
    for pick_index in range(top_count):
        pick = (dest[:, pick_index][:, None] == slot_ids[None, :]).astype(jnp.bfloat16)
        picked_out = jnp.dot(pick, returned, preferred_element_type=jnp.float32)
        expert_sum = expert_sum + route_weight[:, pick_index : pick_index + 1] * picked_out
    return expert_sum.astype(jnp.bfloat16)


def solution(mesh):
    in_specs = (
        P("sp", "tp"),
        P("tp"),
        P("tp", None, None),
        P("tp"),
        P(),
        P(("sp", "tp"), None),
        P(("sp", "tp"), None),
        P("sp", None, "tp"),
        P("sp", None, "tp"),
        P("sp", "tp", None),
    )
    out_specs = P(("sp", "tp"), None)
    return jax.shard_map(
        per_device, mesh=mesh, in_specs=in_specs, out_specs=out_specs, check_vma=False
    )
```

time: 203 us -> 140 us (0.69)
  blocking collectives: 115 us -> 0 us
  Pallas kernels: 0 us -> 95.5 us
  matrix products: 32.1 us -> 7.49 us
  waiting for transfers between devices: 23.9 us -> 8.28 us
  other arithmetic: 9.91 us -> 7.4 us
  starting transfers between devices: 18.4 us -> 15.9 us
  local copies, waits for them, and re-layouts: 2.65 us -> 5 us
    all_to_all x2 -> x0, blocking collectives: 115 us -> none  [the longest x1 63 us: per_device(): lax.all_to_all(copies, ('sp', 'tp'), split_axis=0, concat_axis=0, tiled=T...]
    pallas_call x0 -> x1, Pallas kernels: none -> 95.5 us  [run_experts(): pl.pallas_call(experts_kernel, name='experts', out_shape=jax.ShapeDtypeSt...]
    dot_general x5 -> x2, matrix products: 29.4 us -> 3.83 us  [per_device(): picked_out = jnp.dot(pick, returned, preferred_element_type=jnp.float32)]
    all_to_all x2 -> x1, waiting for transfers between devices: 22.7 us -> 7.69 us  [per_device(): lax.all_to_all(doubled, 'tp', split_axis=0, concat_axis=0, tiled=True)]
    all_to_all x2 -> x1, starting transfers between devices: 8.33 us -> 3.47 us  [per_device(): lax.all_to_all(doubled, 'tp', split_axis=0, concat_axis=0, tiled=True)]
    reduce_sum x2, other arithmetic: 4.42 us -> 0.34 us  [slots_of(): slot = jnp.sum(rank * is_expert, axis=1)]
    ppermute x0 -> x1, starting transfers between devices: none -> 3.02 us  [per_device(): routes_across = lax.ppermute(routes, 'tp', across)]
  transfers between devices with their start and end apart: 4 -> 4, of which waited for: 3 -> 2; matrix products, arithmetic and copies ran while one was open for 2% -> 5% of each run, Pallas kernels for 0% -> 0%
where the time goes in v1:
time: 140 us
  Pallas kernels  95.5 us (68%)
  starting transfers between devices  15.9 us (11%)
  waiting for transfers between devices  8.28 us (6%)
  matrix products  7.49 us (5%)
  other arithmetic  7.4 us (5%)
  local copies, waits for them, and re-layouts  5 us (4%)
    pallas_call x1, Pallas kernels, run_experts(): pl.pallas_call(experts_kernel, name='experts', out_shape=jax.ShapeDtypeSt...  95.5 us
    all_to_all x1, waiting for transfers between devices, per_device(): lax.all_to_all(doubled, 'tp', split_axis=0, concat_axis=0, tiled=True)  7.69 us
    all_to_all x1, starting transfers between devices, sent_to_all(): return lax.all_to_all(copies, axis, split_axis=0, concat_axis=0, tiled=True)  4.83 us
    ppermute x1, starting transfers between devices, passed_along(): return lax.ppermute(block, axis, route)  4.61 us
    dot_general x2, matrix products, per_device(): picked_out = jnp.dot(pick, returned, preferred_element_type=jnp.float32)  3.83 us
    all_to_all x1, starting transfers between devices, per_device(): lax.all_to_all(doubled, 'tp', split_axis=0, concat_axis=0, tiled=True)  3.47 us
    ppermute x1, starting transfers between devices, per_device(): routes_across = lax.ppermute(routes, 'tp', across)  3.02 us
  transfers between devices with their start and end apart: 4, of which 2 were waited for; matrix products, arithmetic and copies ran while one was open for 5% of the time, Pallas kernels for 0%

profile of v1, /device:TPU:1, one launch (start us, length us, event | category | flops | bytes accessed | tf_op | source)
XLA Modules:
  0.0 139.9 jit_solution(17493988091267270213)
XLA Ops:
  0.0 1.1 fusion.10
  1.1 0.6 broadcast_in_dim.10
  1.7 4.8 %all-to-all-start = ((f32[4,1,256]{2,1,0:T(1,128)}), f32[4,1,256]{2,1,0:T(1,128)S(1)}, u32[]{:S(2)}, u32[]{:S(2)}) async-start(f32[4,1,256]{2,1,0:T(1,128)} %broadcast_in_dim.10), calls=%async_computation | async-start | bytes 8192 | tf_op jit(solution)/shard_map/all_to_all | solution.py:25
  6.6 0.8 copy.94
  7.3 3.0 %collective-permute-start.1 = (s32[64,2]{1,0:T(8,128)S(1)}, s32[64,2]{1,0:T(8,128)S(1)}, u32[]{:S(2)}, u32[]{:S(2)}) collective-permute-start(s32[64,2]{1,0:T(8,128)S(1)} %copy.94), channel_id=1, source_target_pairs={{0,2},{1,3},{2,0},{3,1},{4,6},{5,7},{6,4},{7,5},{8,10},{9,11},{10,... | collective-permute-start | bytes 1544 | tf_op jit(solution)/shard_map/ppermute | solution.py:298
  10.4 0.7 broadcast_compare_fusion
  11.2 0.8 slice_bitcast_fusion
  12.4 0.2 reduce_window_sum.17
  12.5 0.2 select_reduce_fusion.1
  13.0 0.2 slice_reduce_fusion
  13.2 0.7 convert_element_type.65
  13.9 0.7 convert_element_type.70
  14.6 0.7 convert_element_type.78
  15.3 0.1 eq.149
  15.5 1.1 fusion.12
  16.6 4.6 %collective-permute-start = (bf16[15,512]{1,0:T(8,128)(2,1)S(1)}, bf16[15,512]{1,0:T(8,128)(2,1)S(1)}, u32[]{:S(2)}, u32[]{:S(2)}) collective-permute-start(bf16[15,512]{1,0:T(8,128)(2,1)S(1)} %slice.46), channel_id=1, source_target_pairs={{0,4},{4,8},{8,12},{12,16},{16,20},{20,24},{24,28},{28,32},{32,36}... | collective-permute-start | bytes 46088 | tf_op jit(solution)/shard_map/ppermute | solution.py:35
  21.3 0.2 reduce_window_sum.18
  21.5 0.6 collective-permute-done
  22.1 1.5 %fusion.5 = bf16[256,512]{1,0:T(8,128)(2,1)S(1)} fusion(bf16[256,512]{1,0:T(8,128)(2,1)} %param.10, bf16[1,512,512]{2,1,0:T(8,128)(2,1)S(1)} %copy-done, bf16[256,512]{1,0:T(8,128)(2,1)S(1)} %fusion.12, bf16[15,512]{1,0:T(8,128)(2,1)S(1)} %collective-permute-done, f32[512]{0:T(512)S(1)} %convert_element_type.70, f32[256]{0:T(256)S(1)} %get-tuple-element.16, ...), kind=kOutput, calls=%fused_computation.12 | convolution fusion | flops 207139840 | bytes 1331264 | tf_op jit(solution)/shard_map/dot_general | solution.py:318
  23.7 0.8 pad_maximum_fusion
  24.5 3.5 %all-to-all-start.1 = ((bf16[4,2,64,512]{3,2,1,0:T(8,128)(2,1)}), bf16[4,2,64,512]{3,2,1,0:T(8,128)(2,1)S(1)}, u32[]{:S(2)}, u32[]{:S(2)}) async-start(bf16[4,2,64,512]{3,2,1,0:T(8,128)(2,1)} %pad_maximum_fusion), calls=%async_computation.1 | async-start | bytes 1048576 | tf_op jit(solution)/shard_map/all_to_all | solution.py:324
  28.0 0.2 select_reduce_fusion
  28.7 7.7 %all-to-all-done.1 = bf16[4,2,64,512]{3,2,1,0:T(8,128)(2,1)S(1)} async-done(((bf16[4,2,64,512]{3,2,1,0:T(8,128)(2,1)}), bf16[4,2,64,512]{3,2,1,0:T(8,128)(2,1)S(1)}, u32[]{:S(2)}, u32[]{:S(2)}) %all-to-all-start.1) | async-done | bytes 524320 | tf_op jit(solution)/shard_map/all_to_all | solution.py:324
  36.5 0.7 copy.113
  37.2 0.2 fusion.7
  37.5 0.3 copy.131
  37.8 0.3 copy.93
  38.2 0.2 copy.130
  38.4 2.1 %convolution_convert_fusion = bf16[512,2048]{1,0:T(8,128)(2,1)} fusion(f32[128,2048]{1,0:T(8,128)S(1)} %bitcast.29, f32[2048]{0:T(1024)S(1)} %convert_element_type.78, f32[128]{0:T(128)S(1)} %rsqrt.20, pred[512,64]{0,1:T(8,128)(4,1)S(1)} %get-tuple-element.19, pred[512,64]{0,1:T(8,128)(4,1)S(1)} %get-tuple-element.18), kind=kOutput, calls=%fused_computation | convolution fusion | flops 270336000 | bytes 3219968 | tf_op jit(solution)/shard_map/dot_general | solution.py:343
  40.5 95.5 %experts.1 = bf16[32,8,2048]{2,1,0:T(8,128)(2,1)} custom-call(bf16[32,16,2048]{2,1,0:T(8,128)(2,1)} %bitcast.28, bf16[1,2048,1792]{2,1,0:T(8,128)(2,1)} %wg_hbm.1, bf16[1,2048,1792]{2,1,0:T(8,128)(2,1)} %wu_hbm.1, bf16[1,1792,2048]{2,1,0:T(8,128)(2,1)} %wd_hbm.1), custom_call_target="tpu_custom_call" | custom-call | tf_op jit(solution)/shard_map/experts/pallas_call | solution.py:251
  136.0 1.6 %fusion.1 = f32[64,2048]{1,0:T(8,128)S(1)} fusion(f32[64,2048]{1,0:T(8,128)S(1)} %bitcast.32, bf16[32,8,2048]{2,1,0:T(8,128)(2,1)} %experts.1, f32[64]{0:T(128)S(1)} %get-tuple-element.14, s32[64]{0:T(128)S(1)} %get-tuple-element.6), kind=kOutput, calls=%fused_computation.4 | convolution fusion | flops 67387392 | bytes 2097664 | tf_op jit(solution)/shard_map/dot_general | solution.py:355
  137.6 2.3 %fusion.2 = bf16[64,2048]{1,0:T(8,128)(2,1)} fusion(f32[64,2048]{1,0:T(8,128)S(1)} %fusion.1, bf16[32,8,2048]{2,1,0:T(8,128)(2,1)} %experts.1, f32[64]{0:T(128)S(1)} %get-tuple-element.13, s32[64]{0:T(128)S(1)} %get-tuple-element.5), kind=kOutput, calls=%fused_computation.5 | convolution fusion | flops 67518464 | bytes 1835520 | tf_op jit(solution)/shard_map/dot_general | solution.py:355
  (29 shorter events, 1.8 us)
Async XLA Ops:
  0.0 22.1 %copy-start = (bf16[1,512,512]{2,1,0:T(8,128)(2,1)S(1)}, bf16[1,512,512]{2,1,0:T(8,128)(2,1)}, u32[]{:S(2)}) copy-start(bf16[1,512,512]{2,1,0:T(8,128)(2,1)} %param.12) | copy-start | bytes 1572868
  1.7 13.8 %all-to-all-start = ((f32[4,1,256]{2,1,0:T(1,128)}), f32[4,1,256]{2,1,0:T(1,128)S(1)}, u32[]{:S(2)}, u32[]{:S(2)}) async-start(f32[4,1,256]{2,1,0:T(1,128)} %broadcast_in_dim.10), calls=%async_computation | async-start | bytes 8192 | tf_op jit(solution)/shard_map/all_to_all | solution.py:25
  7.3 8.0 %collective-permute-start.1 = (s32[64,2]{1,0:T(8,128)S(1)}, s32[64,2]{1,0:T(8,128)S(1)}, u32[]{:S(2)}, u32[]{:S(2)}) collective-permute-start(s32[64,2]{1,0:T(8,128)S(1)} %copy.94), channel_id=1, source_target_pairs={{0,2},{1,3},{2,0},{3,1},{4,6},{5,7},{6,4},{7,5},{8,10},{9,11},{10,... | collective-permute-start | bytes 1544 | tf_op jit(solution)/shard_map/ppermute | solution.py:298
  16.6 5.5 %collective-permute-start = (bf16[15,512]{1,0:T(8,128)(2,1)S(1)}, bf16[15,512]{1,0:T(8,128)(2,1)S(1)}, u32[]{:S(2)}, u32[]{:S(2)}) collective-permute-start(bf16[15,512]{1,0:T(8,128)(2,1)S(1)} %slice.46), channel_id=1, source_target_pairs={{0,4},{4,8},{8,12},{12,16},{16,20},{20,24},{24,28},{28,32},{32,36}... | collective-permute-start | bytes 46088 | tf_op jit(solution)/shard_map/ppermute | solution.py:35
  24.5 11.8 %all-to-all-start.1 = ((bf16[4,2,64,512]{3,2,1,0:T(8,128)(2,1)}), bf16[4,2,64,512]{3,2,1,0:T(8,128)(2,1)S(1)}, u32[]{:S(2)}, u32[]{:S(2)}) async-start(bf16[4,2,64,512]{3,2,1,0:T(8,128)(2,1)} %pad_maximum_fusion), calls=%async_computation.1 | async-start | bytes 1048576 | tf_op jit(solution)/shard_map/all_to_all | solution.py:324

commit v2 on v0

v2 whole, which is shorter than its diff:
```python
import functools

import jax
import jax.numpy as jnp
from jax import lax
from jax.experimental import pallas as pl
from jax.experimental.pallas import tpu as pltpu
from jax.sharding import PartitionSpec as P

NORM_EPS = 1e-06
MESH = pl.DeviceIdType.MESH
F32, BF16 = jnp.float32, jnp.bfloat16
COMBOS = (
    (0, 0), (0, 1),
    (0, 3), (1, 0), (3, 0), (1, 1),
    (3, 3), (1, 3), (3, 1), (0, 2),
    (2, 0), (1, 2), (2, 1), (3, 2),
    (2, 3), (2, 2),
)
ORDER = tuple((dz, dy, dc) for dz, dy in COMBOS for dc in (0, 1))
PEERS = len(ORDER)
CHUNKS = (4, 8, 8, 8, 4)
BASES = tuple(sum(CHUNKS[:c]) for c in range(len(CHUNKS)))
LAST = len(CHUNKS) - 1
CAP = 8
UP, DOWN, COLS = 896, 512, 512


def layer_kernel(
    stream_hbm, mix_gain_hbm, pool_weight_hbm, pool_scale_hbm, ffn_gain_hbm,
    routes_hbm, weights_hbm, wg_hbm, wu_hbm, wd_hbm,
    out_ref,
    stream, mix_gain, pool_weight, pool_scale, ffn_gain, routes, weights, far_routes,
    row_sums, peer_sums, edge_sums, edge_rows, mixed, taken, picks, back, send,
    own, other, wg, wu, wd, hid, part, relay_l, relay_r, from_l, from_r, sums, returned,
    in_sem, w_sem, f_ssem, f_rsem, m_ssem, m_rsem, d_ssem, d_rsem,
    g_ssem, g_rsem, p_ssem, p_rsem, r_ssem, r_rsem,
):
    sp = lax.axis_index("sp")
    tp = lax.axis_index("tp")
    z, y, core = sp // 8, sp // 2 % 4, sp % 2
    left, right, far = (sp, (tp + 3) % 4), (sp, (tp + 1) % 4), (sp, (tp + 2) % 4)
    onward, behind = (sp + 1) % PEERS, (sp + PEERS - 1) % PEERS
    tok_rows, group = stream.shape
    block_rows = tok_rows // 4
    width = out_ref.shape[1]
    up_tiles, down_tiles = wg.shape[0], wd.shape[0]

    def peer_sp(k, sign):
        dz, dy, dc = ORDER[k]
        if sign < 0:
            dz, dy = (4 - dz) % 4, (4 - dy) % 4
        return ((z + dz) % 4) * 8 + ((y + dy) % 4) * 2 + (core + dc) % 2

    barrier = pltpu.get_barrier_semaphore()
    greeted = [(peer_sp(k, 1), tp) for k in range(1, PEERS)] + [left, right, far]
    greeted += [(s, (tp + d) % 4) for s in (onward, behind) for d in (1, 2, 3)]
    for target in greeted:
        pl.semaphore_signal(barrier, inc=1, device_id=target, device_id_type=MESH)

    loads = [
        pltpu.make_async_copy(src, dst, in_sem.at[i])
        for i, (src, dst) in enumerate(
            (
                (stream_hbm, stream), (routes_hbm, routes), (weights_hbm, weights),
                (mix_gain_hbm, mix_gain), (pool_scale_hbm, pool_scale), (ffn_gain_hbm, ffn_gain),
                (pool_weight_hbm, pool_weight),
            )
        )
    ]
    for copy in loads:
        copy.start()
    w_up_copies = [
        pltpu.make_async_copy(
            src.at[0, :, pl.ds(j * UP, UP)], dst.at[j], w_sem.at[2 * j + i]
        )
        for j in range(up_tiles)
        for i, (src, dst) in enumerate(((wg_hbm, wg), (wu_hbm, wu)))
    ]
    w_down_copies = [
        pltpu.make_async_copy(
            wd_hbm.at[0, :, pl.ds(j * DOWN, DOWN)], wd.at[j], w_sem.at[2 * up_tiles + j]
        )
        for j in range(down_tiles)
    ]
    for copy in w_up_copies + w_down_copies:
        copy.start()

    sent = []

    def remote(src, dst, ssem, rsem, target):
        copy = pltpu.make_async_remote_copy(
            src_ref=src, dst_ref=dst, send_sem=ssem, recv_sem=rsem,
            device_id=target, device_id_type=MESH,
        )
        sent.append(copy)
        return copy

    for copy in loads[:3]:
        copy.wait()
    square = stream[...].astype(F32)
    square = square * square
    high = square.astype(BF16)
    low = (square - high.astype(F32)).astype(BF16)
    ones = jnp.ones((8, group), BF16)
    lanes = (((1,), (1,)), ((), ()))
    row_sums[...] = lax.dot_general(
        ones, high, lanes, preferred_element_type=F32
    ) + lax.dot_general(ones, low, lanes, preferred_element_type=F32)

    pl.semaphore_wait(barrier, len(greeted))

    edge = remote(
        stream.at[pl.ds(tok_rows - 16, 16)], edge_rows, f_ssem.at[7], f_rsem.at[7], (onward, tp)
    )
    spread = [
        remote(row_sums, peer_sums.at[d - 1], f_ssem.at[d - 1], f_rsem.at[d - 1], (sp, (tp + d) % 4))
        for d in (1, 2, 3)
    ]
    edge_spread = [
        remote(
            row_sums.at[:, pl.ds(tok_rows - 128, 128)], edge_sums.at[d],
            f_ssem.at[3 + d], f_rsem.at[3 + d], (onward, (tp + d) % 4),
        )
        for d in range(4)
    ]
    swap = remote(routes, far_routes, f_ssem.at[8], f_rsem.at[8], far)
    for copy in spread + edge_spread + [edge, swap]:
        copy.start()
    for copy in loads[3:]:
        copy.wait()

    position = lax.broadcasted_iota(jnp.int32, (tok_rows, 1), 0)
    window = jnp.left_shift(jnp.int32(2), tp)
    lag = position - lax.broadcasted_iota(jnp.int32, (tok_rows, tok_rows), 1)
    band = jnp.where((lag >= 0) & (lag < window), 1.0, 0.0).astype(BF16)
    edge_lag = position[:16] + 16 - lax.broadcasted_iota(jnp.int32, (16, 16), 1)
    edge_limit = jnp.where(sp == 0, 0, window)
    edge_band = jnp.where(edge_lag < edge_limit, 1.0, 0.0).astype(BF16)
    count = jnp.minimum(position + sp * tok_rows + 1, window).astype(F32)

    def row_scale(total):
        scale = lax.rsqrt(total[0:1] / width + NORM_EPS)
        return jnp.broadcast_to(scale, (128, total.shape[1])).T[:, 0:1]

    gain = mix_gain[...].reshape(1, group).astype(F32)
    for copy in spread:
        copy.wait_recv()
    total = row_sums[...] + peer_sums[0] + peer_sums[1] + peer_sums[2]
    normed = (stream[...].astype(F32) * row_scale(total) * gain).astype(BF16)
    window_sum = jnp.dot(band, normed, preferred_element_type=F32)
    for copy in edge_spread + [edge]:
        copy.wait_recv()
    edge_total = edge_sums[0] + edge_sums[1] + edge_sums[2] + edge_sums[3]
    edge_normed = (edge_rows[...].astype(F32) * row_scale(edge_total)[112:] * gain).astype(BF16)
    first = window_sum[:16] + jnp.dot(edge_band, edge_normed, preferred_element_type=F32)
    window_sum = jnp.concatenate([first, window_sum[16:]], axis=0)
    pooled = (window_sum / count - normed.astype(F32)).astype(BF16)
    grouped = jnp.dot(pooled, pool_weight[0], preferred_element_type=F32)
    grouped = grouped * pool_scale[...].reshape(1, group).astype(F32)
    after = (stream[...].astype(F32) + grouped).astype(BF16)
    mixed[...] = after.reshape(4, block_rows, group)

    exchange = []
    for d in (2, 1, 3):
        to = (tp + d) % 4
        for j in range(2):
            exchange.append(
                remote(
                    mixed.at[(to + 2 * j) % 4], taken.at[tp, j],
                    m_ssem.at[d - 1, j], m_rsem.at[d - 1, j], (sp, to),
                )
            )
            exchange[-1].start()
    for j in range(2):
        taken[tp, j] = mixed[(tp + 2 * j) % 4]

    swap.wait_recv()
    lane = lax.broadcasted_iota(jnp.int32, (1, 128), 1)
    first_route, second_route = (
        jnp.concatenate([routes[i : i + 1], far_routes[i : i + 1]], axis=1) for i in range(2)
    )
    weight = jnp.concatenate([weights[...], jnp.zeros((2, 64), F32)], axis=1)
    row = lax.broadcasted_iota(jnp.int32, (PEERS, 128), 0)
    expert = jnp.zeros((PEERS, 128), jnp.int32)
    for k in range(PEERS):
        expert = jnp.where(row == k, peer_sp(k, 1), expert)
    is_first = jnp.where(expert == first_route, 1.0, 0.0)
    is_second = jnp.where(expert == second_route, 1.0, 0.0)
    named = is_first + is_second
    before = lax.broadcasted_iota(jnp.int32, (128, 128), 0)
    token = lax.broadcasted_iota(jnp.int32, (128, 128), 1)
    earlier = jnp.where((before < token) & (before // 64 == token // 64), 1.0, 0.0).astype(BF16)
    rank = jnp.dot(named.astype(BF16), earlier, preferred_element_type=F32)
    slot = jnp.where(named > 0.0, rank + jnp.where(lane >= 64, 8.0, 0.0), -1.0)
    share_of = is_first * weight[0:1] + is_second * weight[1:2]
    slots16 = lax.broadcasted_iota(jnp.int32, (16, 128), 0).astype(F32)
    for k in range(PEERS):
        hit = slot[k : k + 1] == slots16
        picks[k * 16 : (k + 1) * 16] = jnp.where(hit, 1.0, 0.0).astype(BF16)
        back[k * 8 : (k + 1) * 8] = jnp.where(hit[:8], share_of[k : k + 1], 0.0)

    for copy in exchange:
        copy.wait_recv()

    squares = jnp.zeros((2 * block_rows, 1), F32)
    for g in range(4):
        rows = taken[g].reshape(2 * block_rows, group).astype(F32)
        squares = squares + jnp.sum(rows * rows, axis=1, keepdims=True)
    ffn_scale = lax.rsqrt(squares / width + NORM_EPS)
    ffn_gain_row = ffn_gain[...].reshape(1, width).astype(F32)
    for g in range(4):
        cols = pl.ds(g * group, group)
        rows = taken[g].reshape(2 * block_rows, group).astype(F32)
        rows = (rows * ffn_scale * ffn_gain_row[:, g * group : (g + 1) * group]).astype(BF16)
        picked = jnp.dot(picks[...], rows, preferred_element_type=F32)
        send[:, :, cols] = picked.reshape(PEERS, 16, group).astype(BF16)

    dispatch = {}
    for k in range(1, PEERS):
        dispatch[k] = remote(
            send.at[k], own.at[k], d_ssem.at[k], d_rsem.at[k], (peer_sp(k, 1), tp)
        )
        dispatch[k].start()
    own[0] = send[0]

    def arrived(c):
        for k in range(BASES[c], BASES[c] + CHUNKS[c]):
            if k:
                dispatch[k].wait_recv()

    shared = {}

    def share(c):
        half = CHUNKS[c] // 2
        shared[c] = []
        for i, target in enumerate((left, right)):
            places = pl.ds(BASES[c] + i * half, half)
            shared[c].append(
                remote(own.at[places], other.at[places], g_ssem.at[c, i], g_rsem.at[c, i], target)
            )
            shared[c][-1].start()

    def up(c):
        for copy in shared[c]:
            copy.wait_recv()
        if c == 0:
            for copy in w_up_copies:
                copy.wait()
        n, places = CHUNKS[c], pl.ds(BASES[c], CHUNKS[c])

        def tile(j, carry):
            rows = jnp.concatenate(
                [own[places].reshape(n * 16, width), other[places].reshape(n * 16, width)], axis=0
            )
            gate = jnp.dot(rows, wg[j], preferred_element_type=F32)
            raised = jnp.dot(rows, wu[j], preferred_element_type=F32)
            hid[j, : n * 32] = (jax.nn.silu(gate) * raised).astype(BF16)
            return carry

        lax.fori_loop(0, up_tiles, tile, 0)

    def down(c):
        if c == 0:
            for copy in w_down_copies:
                copy.wait()
        n, half = CHUNKS[c], CHUNKS[c] // 2
        span = pl.ds(BASES[c] * CAP, n * CAP)

        def tile(j, carry):
            rows = jnp.concatenate([hid[i, : n * 32] for i in range(up_tiles)], axis=1)
            out = jnp.dot(rows, wd[j], preferred_element_type=F32)
            out = out.reshape(2, n, 2, CAP, DOWN)
            mine, others = out[0], out[1]
            cols = pl.ds(pl.multiple_of(j * DOWN, DOWN), DOWN)
            blocks = (
                mine[:, 0],
                mine[:, 1],
                jnp.concatenate([others[:half, 0], others[half:, 1]], axis=0),
                jnp.concatenate([others[:half, 1], others[half:, 0]], axis=0),
            )
            for b, block in enumerate(blocks):
                part[b, span, cols] = block.reshape(n * CAP, DOWN).astype(BF16)
            return carry

        lax.fori_loop(0, down_tiles, tile, 0)

    moves = {}

    def halves(c):
        half = CHUNKS[c] // 2 * CAP
        base = BASES[c] * CAP
        return pl.ds(base, half), pl.ds(base + half, half), pl.ds(base // 2, half)

    def reduce_first(c):
        head, tail, via = halves(c)
        plan = (
            (1, head, relay_l, via, right),
            (1, tail, relay_r, via, left),
            (2, tail, from_l, tail, right),
            (3, head, from_r, head, left),
            (2, head, from_l, head, right),
            (3, tail, from_r, tail, left),
        )
        moves[c] = [
            remote(part.at[b, src], buffer.at[dst], p_ssem.at[c, i], p_rsem.at[c, i], target)
            for i, (b, src, buffer, dst, target) in enumerate(plan)
        ]
        for copy in moves[c][:4]:
            copy.start()

    def reduce_second(c):
        head, tail, via = halves(c)
        moves[c][0].wait_recv()
        moves[c][1].wait_recv()
        for j in range(width // COLS):
            cols = pl.ds(j * COLS, COLS)
            for b, rows, relay in ((2, head, relay_l), (3, tail, relay_r)):
                total = part[b, rows, cols].astype(F32) + relay[via, cols].astype(F32)
                part[b, rows, cols] = total.astype(BF16)
        moves[c][4].start()
        moves[c][5].start()

    returns = {}

    def reduce_third(c):
        for copy in moves[c][2:]:
            copy.wait_recv()
        n = CHUNKS[c]
        span, places = pl.ds(BASES[c] * CAP, n * CAP), pl.ds(BASES[c], n)
        for j in range(width // COLS):
            cols = pl.ds(j * COLS, COLS)
            total = part[0, span, cols].astype(F32) + from_l[span, cols].astype(F32)
            total = total + from_r[span, cols].astype(F32)
            sums[places, :, cols] = total.reshape(n, CAP, COLS).astype(BF16)
        for k in range(BASES[c], BASES[c] + n):
            if k:
                returns[k] = remote(
                    sums.at[k], returned.at[pl.ds(k * CAP, CAP)],
                    r_ssem.at[k], r_rsem.at[k], (peer_sp(k, -1), tp),
                )
                returns[k].start()
            else:
                returned[0:CAP] = sums[0]

    for c in range(2):
        arrived(c)
        share(c)
    spread_weight = back[...].T[:block_rows]
    weight_high = spread_weight.astype(BF16)
    weight_low = (spread_weight - weight_high.astype(F32)).astype(BF16)
    combine = jnp.concatenate([weight_high, weight_low], axis=0)
    picks[: 2 * block_rows] = combine[:, :128]
    picks[2 * block_rows : 4 * block_rows] = combine[:, 128:]
    for c in range(len(CHUNKS)):
        up(c)
        if c + 2 < len(CHUNKS):
            arrived(c + 2)
            share(c + 2)
        if c:
            reduce_second(c - 1)
        down(c)
        reduce_first(c)
        if c:
            reduce_third(c - 1)
    reduce_second(LAST)
    reduce_third(LAST)
    for k in range(1, PEERS):
        returns[k].wait_recv()
    combine = jnp.concatenate(
        [picks[: 2 * block_rows], picks[2 * block_rows : 4 * block_rows]], axis=1
    )
    for g in range(4):
        cols = pl.ds(g * group, group)
        gained = jnp.dot(combine, returned[:, cols], preferred_element_type=F32)
        gained = gained[:block_rows] + gained[block_rows:]
        out_ref[:, cols] = (taken[g, 0].astype(F32) + gained).astype(BF16)
    for copy in sent:
        copy.wait_send()


def per_device(
    stream, mix_gain, pool_weight, pool_scale, ffn_gain, routes, route_weight, w_gate, w_up, w_down
):
    tok_rows, group = stream.shape
    width, inner = w_gate.shape[1:]
    block_rows = tok_rows // 4
    up_tiles, down_tiles = inner // UP, width // DOWN
    dma = pltpu.SemaphoreType.DMA
    slots = PEERS * CAP
    return pl.pallas_call(
        layer_kernel,
        name="experts",
        out_shape=jax.ShapeDtypeStruct((block_rows, width), BF16),
        in_specs=[pl.BlockSpec(memory_space=pltpu.HBM)] * 10,
        out_specs=pl.BlockSpec(memory_space=pltpu.VMEM),
        scratch_shapes=[
            pltpu.VMEM((tok_rows, group), BF16),
            pltpu.VMEM((group,), BF16),
            pltpu.VMEM((1, group, group), BF16),
            pltpu.VMEM((group,), BF16),
            pltpu.VMEM((width,), BF16),
            pltpu.VMEM((2, block_rows), jnp.int32),
            pltpu.VMEM((2, block_rows), F32),
            pltpu.VMEM((2, block_rows), jnp.int32),
            pltpu.VMEM((8, tok_rows), F32),
            pltpu.VMEM((3, 8, tok_rows), F32),
            pltpu.VMEM((4, 8, 128), F32),
            pltpu.VMEM((16, group), BF16),
            pltpu.VMEM((4, block_rows, group), BF16),
            pltpu.VMEM((4, 2, block_rows, group), BF16),
            pltpu.VMEM((PEERS * 16, 128), BF16),
            pltpu.VMEM((slots, 128), F32),
            pltpu.VMEM((PEERS, 16, width), BF16),
            pltpu.VMEM((PEERS, 16, width), BF16),
            pltpu.VMEM((PEERS, 16, width), BF16),
            pltpu.VMEM((up_tiles, width, UP), BF16),
            pltpu.VMEM((up_tiles, width, UP), BF16),
            pltpu.VMEM((down_tiles, inner, DOWN), BF16),
            pltpu.VMEM((up_tiles, max(CHUNKS) * 32, UP), BF16),
            pltpu.VMEM((4, slots, width), BF16),
            pltpu.VMEM((slots // 2, width), BF16),
            pltpu.VMEM((slots // 2, width), BF16),
            pltpu.VMEM((slots, width), BF16),
            pltpu.VMEM((slots, width), BF16),
            pltpu.VMEM((PEERS, CAP, width), BF16),
            pltpu.VMEM((slots, width), BF16),
            dma((7,)),
            dma((2 * up_tiles + down_tiles,)),
            dma((9,)), dma((9,)),
            dma((3, 2)), dma((3, 2)),
            dma((PEERS,)), dma((PEERS,)),
            dma((len(CHUNKS), 2)), dma((len(CHUNKS), 2)),
            dma((len(CHUNKS), 6)), dma((len(CHUNKS), 6)),
            dma((PEERS,)), dma((PEERS,)),
        ],
        compiler_params=pltpu.CompilerParams(
            collective_id=0, has_side_effects=True, vmem_limit_bytes=62 * 2**20
        ),
    )(
        stream, mix_gain, pool_weight, pool_scale, ffn_gain,
        routes.T, route_weight.T, w_gate, w_up, w_down,
    )


def solution(mesh):
    in_specs = (
        P("sp", "tp"),
        P("tp"),
        P("tp", None, None),
        P("tp"),
        P(),
        P(("sp", "tp"), None),
        P(("sp", "tp"), None),
        P("sp", None, "tp"),
        P("sp", None, "tp"),
        P("sp", "tp", None),
    )
    out_specs = P(("sp", "tp"), None)
    return jax.shard_map(
        per_device, mesh=mesh, in_specs=in_specs, out_specs=out_specs, check_vma=False
    )
```

time: 203 us -> 107 us (0.53)
  blocking collectives: 115 us -> 0 us
  Pallas kernels: 0 us -> 105 us
  matrix products: 32.1 us -> 0 us
  waiting for transfers between devices: 23.9 us -> 0 us
  starting transfers between devices: 18.4 us -> 0 us
  other arithmetic: 9.91 us -> 0 us
    all_to_all x2 -> x0, blocking collectives: 115 us -> none  [the longest x1 63 us: per_device(): lax.all_to_all(copies, ('sp', 'tp'), split_axis=0, concat_axis=0, tiled=T...]
    pallas_call x0 -> x1, Pallas kernels: none -> 105 us  [per_device(): pl.pallas_call(layer_kernel, name='experts', out_shape=jax.ShapeDtypeStru...]
    dot_general x7 -> x0, matrix products: 32.1 us -> none  [the longest x1 10.2 us: expert_rows(): up_val = jnp.dot(flat_rows, w_up[0], preferred_element_type=jnp.float32)]
    all_to_all x3 -> x0, waiting for transfers between devices: 23.9 us -> none  [the longest x1 17.1 us: per_device(): lax.all_to_all(served, 'sp', split_axis=0, concat_axis=0, tiled=True)]
    all_to_all x3 -> x0, starting transfers between devices: 13.2 us -> none  [the longest x1 4.92 us: per_device(): lax.all_to_all(served, 'sp', split_axis=0, concat_axis=0, tiled=True)]
    reduce_sum x5 -> x0, other arithmetic: 5.74 us -> none  [the longest x1 4.25 us: sent_and_summed(): return arrived.astype(jnp.float32).sum(axis=0)]
    ppermute x1 -> x0, starting transfers between devices: 5.19 us -> none  [passed_along(): return lax.ppermute(block, axis, route)]
    convert_element_type x6 -> x0, other arithmetic: 3.23 us -> none  [the longest x1 1.08 us: per_device(): (stream_f32 * row_scale * mix_gain.astype(jnp.float32)).astype(jnp.bfloat16)]
  transfers between devices with their start and end apart: 4 -> 0, of which waited for: 3 -> 0; matrix products, arithmetic and copies ran while one was open for 2% -> 0% of each run, Pallas kernels for 0% -> 0%
where the time goes in v2:
time: 107 us; the launch traced here: 106 us
  Pallas kernels  105 us (98%)
  local copies, waits for them, and re-layouts  1.67 us (2%)
    pallas_call x1, Pallas kernels, per_device(): pl.pallas_call(layer_kernel, name='experts', out_shape=jax.ShapeDtypeStru...  105 us

profile of v2, /device:TPU:1, one launch (start us, length us, event | category | flops | bytes accessed | tf_op | source)
XLA Modules:
  0.0 106.5 jit_solution(8091007589720049934)
XLA Ops:
  0.0 104.8 %experts.1 = bf16[64,2048]{1,0:T(8,128)(2,1)} custom-call(bf16[256,512]{1,0:T(8,128)(2,1)} %stream_hbm.1, bf16[512]{0:T(512)(128)(2,1)} %mix_gain_hbm.1, bf16[1,512,512]{2,1,0:T(8,128)(2,1)} %pool_weight_hbm.1, bf16[512]{0:T(512)(128)(2,1)} %pool_scale_hbm.1, bf16[2048]{0:T(1024)(128)(2,1)} %ffn_gain_hbm.1, s32[2,64]{1,0:T(2,128)} %bitcast.2, ...), custom_call_target="tpu_custom_call" | custom-call | tf_op jit(solution)/shard_map/experts/pallas_call | solution.py:391
  104.8 1.7 %copy.12 = bf16[64,2048]{1,0:T(8,128)(2,1)} copy(bf16[64,2048]{1,0:T(8,128)(2,1)} %experts.1) | data formatting | bytes 524288
